TPU v7x, 32 devices: a whole 2x2x4 slice. The times are simulated.
32 devices in a mesh: sp: 8 (over z, x), tp: 4 (over y, core).
Axes of the slice: x: 2, y: 2, z: 4, core: 2. Of those that a mesh axis runs over, the one named last changes fastest.
Arguments:
- cotangent: bfloat16 [1024, 2048], P('sp'), may hold values from -6 to 6
- stream: bfloat16 [1024, 2048], P('sp'), may hold values from -6 to 6
- routes: int32 [1024, 2], P('sp'), may hold values from 0 to 3, all different within a row; in each aligned block of 128 rows (0 to 127, 128 to 255, ...) at most 96 rows name the same one
- route_weights: float32 [1024, 2], P('sp'), may hold values from 0.25 to 1
- gate_weight: bfloat16 [8, 2048, 2048], P('sp', None, 'tp'), may hold values from -0.125 to 0.125
- up_weight: bfloat16 [8, 2048, 2048], P('sp', None, 'tp'), may hold values from -0.125 to 0.125
- down_weight: bfloat16 [8, 2048, 2048], P('sp', 'tp'), may hold values from -0.09375 to 0.09375
- outer_gate: bfloat16 [1024, 1024], P('sp', 'tp'), may hold values from -6 to 6
- inner_gate: bfloat16 [1024, 1024], P('sp', 'tp'), may hold values from -6 to 6
- conv_input: bfloat16 [1024, 1024], P('sp', 'tp'), may hold values from -6 to 6
- conv_taps: bfloat16 [3, 1024], P(None, 'tp'), may hold values from -1 to 1
- out_weight: bfloat16 [2048, 1024], P(None, 'tp'), may hold values from -0.1875 to 0.1875
Outputs:
- gate_grad: bfloat16 [8, 2048, 2048], P('sp', None, 'tp')
- up_grad: bfloat16 [8, 2048, 2048], P('sp', None, 'tp')
- down_grad: bfloat16 [8, 2048, 2048], P('sp', 'tp')
- out_grad: float32 [2048, 1024], P('sp', 'tp')
- outer_grad: bfloat16 [1024, 1024], P('sp', 'tp')
- inner_grad: bfloat16 [1024, 1024], P('sp', 'tp')
- input_grad: bfloat16 [1024, 1024], P('sp', 'tp')
Inputs may be any that keep to these rules, and one draw needn't show every extreme that they name: `routes`: each token names two different experts. Among the 128 tokens of one index of sp no expert is named by more than 96 tokens, a bound that some block of them reaches in every draw.
All inputs are finite; a program needn't handle non-finite values.
Results may differ from a plain program's by a relative error of at most 0.02.
Values may be sent and summed in bfloat16 or wider, within the bound.
A program may use at most 64 MiB of HBM per device.

v0:
```python
import jax
import jax.numpy as jnp
from jax import lax
from jax.sharding import PartitionSpec as P


def from_behind(block, axis, distance):
    devices = range(lax.axis_size(axis))
    route = [(i - distance, i) for i in devices if i - distance in devices]
    return lax.ppermute(block, axis, route)


def per_device(
    cotangent,
    stream,
    routes,
    route_weights,
    gate_weight,
    up_weight,
    down_weight,
    outer_gate,
    inner_gate,
    conv_input,
    conv_taps,
    out_weight,
):
    groups = lax.axis_size("sp")
    tp_count = lax.axis_size("tp")
    experts = groups // 2
    tok_rows = stream.shape[0]
    model_width = stream.shape[1]
    capacity = 3 * tok_rows // experts
    slot_total = experts * capacity
    contract_first = (((0,), (0,)), ((), ()))
    contract_last = (((1,), (1,)), ((), ()))
    flat_routes = routes.reshape(-1)
    choose = (flat_routes[:, None] == jnp.arange(experts, dtype=jnp.int32)[None, :]).astype(
        jnp.int32
    )
    before = jnp.cumsum(choose, axis=0) - choose
    slot_place = flat_routes * capacity + jnp.sum(before * choose, axis=1)
    slot_table = (jnp.arange(slot_total, dtype=jnp.int32)[:, None] == slot_place[None, :]).astype(
        jnp.float32
    )
    select = jnp.sum(slot_table.reshape(slot_total, tok_rows, 2), axis=2).astype(jnp.bfloat16)
    slot_weight = jnp.sum(slot_table * route_weights.reshape(-1)[None, :], axis=1)
    block_width = model_width // tp_count
    offset = lax.axis_index("tp") * block_width
    rows_part = lax.dynamic_slice_in_dim(stream, offset, block_width, 1)
    cot_part = lax.dynamic_slice_in_dim(cotangent, offset, block_width, 1)
    sent_rows = jnp.dot(select, rows_part, preferred_element_type=jnp.float32).astype(jnp.bfloat16)
    sent_cot = (
        jnp.dot(select, cot_part, preferred_element_type=jnp.float32) * slot_weight[:, None]
    ).astype(jnp.bfloat16)
    sent_rows = jnp.repeat(sent_rows.reshape(experts, capacity, -1), 2, axis=0)
    sent_cot = jnp.repeat(sent_cot.reshape(experts, capacity, -1), 2, axis=0)
    recv_rows, recv_cot = (
        lax.all_to_all(sent_rows, "sp", split_axis=0, concat_axis=0, tiled=True),
        lax.all_to_all(sent_cot, "sp", split_axis=0, concat_axis=0, tiled=True),
    )
    recv_rows, recv_cot = (
        lax.all_gather(recv_rows, "tp", axis=2, tiled=True),
        lax.all_gather(recv_cot, "tp", axis=2, tiled=True),
    )
    slots = groups * capacity
    routed_rows = recv_rows.reshape(slots, model_width)
    routed_cot = recv_cot.reshape(slots, model_width)
    gate_local = gate_weight[0]
    up_local = up_weight[0]
    down_local = down_weight[0]
    gate_pre = jnp.dot(routed_rows, gate_local, preferred_element_type=jnp.float32)
    up_pre = jnp.dot(routed_rows, up_local, preferred_element_type=jnp.float32)
    hidden_grad = lax.dot_general(
        routed_cot, down_local, contract_last, preferred_element_type=jnp.float32
    )
    sigma = jax.nn.sigmoid(gate_pre)
    silu_gate = gate_pre * sigma
    hidden = (silu_gate * up_pre).astype(jnp.bfloat16)
    up_delta = (hidden_grad * silu_gate).astype(jnp.bfloat16)
    gate_delta = (hidden_grad * up_pre * sigma * (1.0 + gate_pre * (1.0 - sigma))).astype(
        jnp.bfloat16
    )
    gate_grad = lax.dot_general(
        routed_rows, gate_delta, contract_first, preferred_element_type=jnp.float32
    ).astype(jnp.bfloat16)[None]
    up_grad = lax.dot_general(
        routed_rows, up_delta, contract_first, preferred_element_type=jnp.float32
    ).astype(jnp.bfloat16)[None]
    down_grad = lax.dot_general(
        hidden, routed_cot, contract_first, preferred_element_type=jnp.float32
    ).astype(jnp.bfloat16)[None]
    row_partial = lax.dot_general(
        gate_delta, gate_local, contract_last, preferred_element_type=jnp.float32
    )
    row_partial = row_partial + lax.dot_general(
        up_delta, up_local, contract_last, preferred_element_type=jnp.float32
    )
    half_sums = lax.psum_scatter(
        row_partial.astype(jnp.bfloat16), "tp", scatter_dimension=1, tiled=True
    ).astype(jnp.float32)
    block_width = half_sums.shape[1]
    half_grad = half_sums.reshape(groups, capacity, block_width).astype(jnp.bfloat16)
    returned = lax.all_to_all(half_grad, "sp", split_axis=0, concat_axis=0, tiled=True)
    returned = returned.reshape(experts, 2, capacity, block_width)
    select_three = select.reshape(experts, capacity, tok_rows)
    moe_part = jnp.einsum(
        "ecr,emcd->rd", select_three, returned, preferred_element_type=jnp.float32
    ).astype(jnp.bfloat16)
    moe_grad = lax.all_gather(moe_part, "tp", axis=1, tiled=True)
    stream_grad = (cotangent.astype(jnp.float32) + moe_grad.astype(jnp.float32)).astype(
        jnp.bfloat16
    )
    taps = conv_taps.astype(jnp.float32)
    outer_f = outer_gate.astype(jnp.float32)
    inner_f = inner_gate.astype(jnp.float32)
    input_f = conv_input.astype(jnp.float32)
    mixed = inner_f * input_f
    earlier = from_behind(mixed[-2:], "sp", 1)
    padded = jnp.concatenate([earlier, mixed], axis=0)
    conv_sum = taps[0] * padded[:-2] + taps[1] * padded[1:-1] + taps[2] * padded[2:]
    conv_out = (outer_f * conv_sum).astype(jnp.bfloat16)
    out_grad = lax.psum_scatter(
        lax.dot_general(
            stream_grad, conv_out, contract_first, preferred_element_type=jnp.float32
        ).astype(jnp.bfloat16),
        "sp",
        scatter_dimension=0,
        tiled=True,
    ).astype(jnp.float32)
    conv_grad = jnp.dot(stream_grad, out_weight, preferred_element_type=jnp.float32)
    outer_grad = (conv_grad * conv_sum).astype(jnp.bfloat16)
    scaled = conv_grad * outer_f
    later = from_behind(scaled[:2], "sp", -1)
    extended = jnp.concatenate([scaled, later], axis=0)
    mixed_grad = taps[2] * extended[:-2] + taps[1] * extended[1:-1] + taps[0] * extended[2:]
    inner_grad = (mixed_grad * input_f).astype(jnp.bfloat16)
    input_grad = (mixed_grad * inner_f).astype(jnp.bfloat16)
    return (gate_grad, up_grad, down_grad, out_grad, outer_grad, inner_grad, input_grad)


def solution(mesh):
    placed = (
        P("sp", None),
        P("sp", None),
        P("sp", None),
        P("sp", None),
        P("sp", None, "tp"),
        P("sp", None, "tp"),
        P("sp", "tp", None),
        P("sp", "tp"),
        P("sp", "tp"),
        P("sp", "tp"),
        P(None, "tp"),
        P(None, "tp"),
    )
    return jax.shard_map(
        per_device,
        mesh=mesh,
        in_specs=placed,
        out_specs=(
            P("sp", None, "tp"),
            P("sp", None, "tp"),
            P("sp", "tp", None),
            P("sp", "tp"),
            P("sp", "tp"),
            P("sp", "tp"),
            P("sp", "tp"),
        ),
        check_vma=False,
    )
```

profile of v0, /device:TPU:0, one launch (start us, length us, event | category | flops | bytes accessed | tf_op | source)
XLA Modules:
  0.0 253.2 jit_solution(881290032400397519)
XLA Ops:
  8.5 1.2 reduce-window.6
  11.1 1.2 convolution_convert_fusion.4
  12.4 27.3 %all_to_all.15 = bf16[8,96,512]{2,1,0:T(8,128)(2,1)} all-to-all(bf16[8,96,512]{2,1,0:T(8,128)(2,1)S(1)} %bitcast.73), channel_id=1, replica_groups=mesh['sp'=8,'tp'=4] {'sp'}, dimensions={0} | all-to-all | bytes 1572864 | tf_op jit(solution)/shard_map/all_to_all | solution.py:58
  40.6 23.3 %all_to_all.16 = bf16[8,96,512]{2,1,0:T(8,128)(2,1)} all-to-all(bf16[8,96,512]{2,1,0:T(8,128)(2,1)S(1)} %bitcast.74), channel_id=1, replica_groups=mesh['sp'=8,'tp'=4] {'sp'}, dimensions={0} | all-to-all | bytes 1572864 | tf_op jit(solution)/shard_map/all_to_all | solution.py:59
  63.9 3.5 %all-gather.3.cloned.1.call-done = bf16[8,96,2048]{2,1,0:T(8,128)(2,1)} async-done(((bf16[8,96,512]{2,1,0:T(8,128)(2,1)}), bf16[8,96,2048]{2,1,0:T(8,128)(2,1)}) %all-gather.3.cloned.1.call-update) | async-done | bytes 3145744 | tf_op jit(solution)/shard_map/all_gather | solution.py:62
  67.4 5.0 %fusion.5 = f32[768,512]{1,0:T(8,128)} fusion(bf16[768,2048]{1,0:T(8,128)(2,1)} %bitcast.86, bf16[1,2048,512]{2,1,0:T(8,128)(2,1)S(1)} %copy-done), kind=kOutput, calls=%fused_computation.10 | convolution fusion | flops 1610612736 | bytes 6815744 | tf_op jit(solution)/shard_map/dot_general | solution.py:71
  72.4 2.9 %fusion.8 = f32[768,512]{1,0:T(8,128)} fusion(bf16[768,2048]{1,0:T(8,128)(2,1)S(1)} %bitcast.88, bf16[1,2048,512]{2,1,0:T(8,128)(2,1)S(1)} %copy-done.2), kind=kOutput, calls=%fused_computation.13 | convolution fusion | flops 1610612736 | bytes 6815744 | tf_op jit(solution)/shard_map/dot_general | solution.py:72
  75.3 22.2 %all-gather.5.cloned.1.call-done = bf16[8,96,2048]{2,1,0:T(8,128)(2,1)} async-done(((bf16[8,96,512]{2,1,0:T(8,128)(2,1)}), bf16[8,96,2048]{2,1,0:T(8,128)(2,1)}) %all-gather.5.cloned.1.call-update) | async-done | bytes 3145744 | tf_op jit(solution)/shard_map/all_gather | solution.py:63
  97.5 5.7 %multiply_convert_fusion.1 = (bf16[768,512]{1,0:T(8,128)(2,1)S(1)}, bf16[768,512]{1,0:T(8,128)(2,1)S(1)}) fusion(f32[768,512]{1,0:T(8,128)} %fusion.5, f32[768,512]{1,0:T(8,128)} %fusion.8, bf16[768,2048]{1,0:T(8,128)(2,1)} %bitcast.90, bf16[1,512,2048]{2,1,0:T(8,128)(2,1)} %param.18), kind=kOutput, calls=%fused_computation.19 | convolution fusion | flops 1615724544 | bytes 9961472 | tf_op jit(solution)/shard_map/dot_general | solution.py:73
  103.3 1.8 fusion.3
  105.4 3.5 %add_convert_fusion = bf16[768,2048]{1,0:T(8,128)(2,1)} fusion(f32[768,2048]{1,0:T(8,128)S(1)} %fusion.3, bf16[768,512]{1,0:T(8,128)(2,1)S(1)} %get-tuple-element.11, bf16[1,2048,512]{2,1,0:T(8,128)(2,1)S(1)} %copy-done.3), kind=kOutput, calls=%fused_computation | convolution fusion | flops 1613758464 | bytes 12320768 | tf_op jit(solution)/shard_map/dot_general | solution.py:95
  109.0 37.9 %reduce-scatter.3.cloned.1.call-done = bf16[768,512]{1,0:T(8,128)(2,1)} async-done(((bf16[768,2048]{1,0:T(8,128)(2,1)}), bf16[768,512]{1,0:T(8,128)(2,1)}) %reduce-scatter.3.cloned.1.call-update) | async-done | bytes 786448 | tf_op jit(solution)/shard_map/reduce_scatter | solution.py:98
  146.8 5.5 %all-to-all-start.2 = ((bf16[8,96,512]{2,1,0:T(8,128)(2,1)}), bf16[8,96,512]{2,1,0:T(8,128)(2,1)S(1)}, u32[]{:S(2)}, u32[]{:S(2)}) async-start(bf16[8,96,512]{2,1,0:T(8,128)(2,1)} %bitcast.78), calls=%async_computation.3 | async-start | bytes 1572864 | tf_op jit(solution)/shard_map/all_to_all | solution.py:103
  153.3 3.9 %collective-permute-start = (f32[2,256]{1,0:T(2,128)S(1)}, f32[2,256]{1,0:T(2,128)S(1)}, u32[]{:S(2)}, u32[]{:S(2)}) collective-permute-start(f32[2,256]{1,0:T(2,128)S(1)} %slice.49), channel_id=1, source_target_pairs={{0,4},{4,8},{8,12},{12,16},{16,20},{20,24},{24,28},{1,5},{5,9},{9,... | collective-permute-start | bytes 6152 | tf_op jit(solution)/shard_map/ppermute | solution.py:10
  157.2 15.2 %all-to-all-done.2 = bf16[8,96,512]{2,1,0:T(8,128)(2,1)S(1)} async-done(((bf16[8,96,512]{2,1,0:T(8,128)(2,1)}), bf16[8,96,512]{2,1,0:T(8,128)(2,1)S(1)}, u32[]{:S(2)}, u32[]{:S(2)}) %all-to-all-start.2) | async-done | bytes 786464 | tf_op jit(solution)/shard_map/all_to_all | solution.py:103
  172.8 6.7 %all_gather.11 = bf16[128,2048]{1,0:T(8,128)(2,1)S(1)} all-gather(bf16[128,512]{1,0:T(8,128)(2,1)S(1)} %fusion.14), channel_id=1, replica_groups=mesh['sp'=8,'tp'=4] {'tp'}, dimensions={1}, use_global_device_ids=true | all-gather | bytes 655360 | tf_op jit(solution)/shard_map/all_gather | solution.py:109
  179.5 1.0 multiply_convert_fusion.4
  180.5 1.5 convolution_convert_fusion.3
  182.1 5.2 %fusion = bf16[1,2048,512]{2,1,0:T(8,128)(2,1)} fusion(bf16[768,2048]{1,0:T(8,128)(2,1)} %bitcast.87, bf16[768,512]{1,0:T(8,128)(2,1)S(1)} %copy-done.8), kind=kOutput, calls=%fused_computation.4 | convolution fusion | flops 1611661312 | bytes 6029312 | tf_op jit(solution)/shard_map/dot_general | solution.py:83
  187.3 3.3 %fusion.2 = bf16[1,512,2048]{2,1,0:T(8,128)(2,1)} fusion(bf16[768,2048]{1,0:T(8,128)(2,1)S(1)} %bitcast.91, f32[768,512]{1,0:T(8,128)S(1)} %copy-done.21, f32[768,512]{1,0:T(8,128)S(1)} %copy-done.20), kind=kOutput, calls=%fused_computation.6 | convolution fusion | flops 1614020608 | bytes 8388608 | tf_op jit(solution)/shard_map/dot_general | solution.py:89
  190.6 1.4 collective-permute-start.1
  192.1 3.2 %fusion.1 = bf16[1,2048,512]{2,1,0:T(8,128)(2,1)} fusion(bf16[768,2048]{1,0:T(8,128)(2,1)S(1)} %bitcast.89, bf16[768,512]{1,0:T(8,128)(2,1)S(1)} %copy-done.6), kind=kOutput, calls=%fused_computation.5 | convolution fusion | flops 1611661312 | bytes 6029312 | tf_op jit(solution)/shard_map/dot_general | solution.py:86
  197.6 47.4 %reduce-scatter.5.cloned.1.call-done = bf16[256,256]{1,0:T(8,128)(2,1)} async-done(((bf16[2048,256]{1,0:T(8,128)(2,1)}), bf16[256,256]{1,0:T(8,128)(2,1)}) %reduce-scatter.5.cloned.1.call-update) | async-done | bytes 131088 | tf_op jit(solution)/shard_map/reduce_scatter | solution.py:122
  245.0 1.6 convert_element_type.125
  (84 shorter events, 7.6 us)
Async XLA Ops:
  7.2 60.3 %copy-start = (bf16[1,2048,512]{2,1,0:T(8,128)(2,1)S(1)}, bf16[1,2048,512]{2,1,0:T(8,128)(2,1)}, u32[]{:S(2)}) copy-start(bf16[1,2048,512]{2,1,0:T(8,128)(2,1)} %param.16) | copy-start | bytes 6291460
  7.2 60.3 %all-gather.3.cloned.1.call-start = ((), (), s32[]{:S(2)}) async-start(), calls=%async_computation.5 | async-start | bytes 3932160 | tf_op jit(solution)/shard_map/all_gather | solution.py:62
  11.1 28.7 %copy-start.16 = (f32[128,2]{0,1:T(2,128)S(1)}, f32[128,2]{0,1:T(2,128)}, u32[]{:S(2)}) copy-start(f32[128,2]{0,1:T(2,128)} %param.15) | copy-start | bytes 3076
  11.1 29.1 %copy-start.1 = (bf16[128,2048]{1,0:T(8,128)(2,1)S(1)}, bf16[128,2048]{1,0:T(8,128)(2,1)}, u32[]{:S(2)}) copy-start(bf16[128,2048]{1,0:T(8,128)(2,1)} %param.12) | copy-start | bytes 1572868
  39.7 57.8 %all-gather.5.cloned.1.call-start = ((), (), s32[]{:S(2)}) async-start(), calls=%async_computation.6 | async-start | bytes 3932160 | tf_op jit(solution)/shard_map/all_gather | solution.py:63
  63.9 83.0 %reduce-scatter.3.cloned.1.call-start = ((), (), s32[]{:S(2)}) async-start(), calls=%async_computation.7 | async-start | bytes 3932160 | tf_op jit(solution)/shard_map/reduce_scatter | solution.py:98
  67.4 5.0 %copy-start.2 = (bf16[1,2048,512]{2,1,0:T(8,128)(2,1)S(1)}, bf16[1,2048,512]{2,1,0:T(8,128)(2,1)}, u32[]{:S(2)}) copy-start(bf16[1,2048,512]{2,1,0:T(8,128)(2,1)} %param.17) | copy-start | bytes 6291460
  67.4 5.0 %copy-start.17 = (bf16[8,96,2048]{2,1,0:T(8,128)(2,1)S(1)}, bf16[8,96,2048]{2,1,0:T(8,128)(2,1)}, u32[]{:S(2)}) copy-start(bf16[8,96,2048]{2,1,0:T(8,128)(2,1)} %all-gather.3.cloned.1.call-done) | copy-start | bytes 9437188
  108.9 48.3 %copy-start.15 = (bf16[3,256]{1,0:T(4,128)(2,1)S(1)}, bf16[3,256]{1,0:T(4,128)(2,1)}, u32[]{:S(2)}) copy-start(bf16[3,256]{1,0:T(4,128)(2,1)} %param.22) | copy-start | bytes 4612
  146.8 25.6 %all-to-all-start.2 = ((bf16[8,96,512]{2,1,0:T(8,128)(2,1)}), bf16[8,96,512]{2,1,0:T(8,128)(2,1)S(1)}, u32[]{:S(2)}, u32[]{:S(2)}) async-start(bf16[8,96,512]{2,1,0:T(8,128)(2,1)} %bitcast.78), calls=%async_computation.3 | async-start | bytes 1572864 | tf_op jit(solution)/shard_map/all_to_all | solution.py:103
  152.4 92.7 %reduce-scatter.5.cloned.1.call-start = ((), (), s32[]{:S(2)}) async-start(), calls=%async_computation.8 | async-start | bytes 1179648 | tf_op jit(solution)/shard_map/reduce_scatter | solution.py:122
  153.3 3.9 %copy-start.10 = (f32[128,256]{1,0:T(8,128)}, f32[128,256]{1,0:T(8,128)S(1)}, u32[]{:S(2)}) copy-start(f32[128,256]{1,0:T(8,128)S(1)} %convert_multiply_fusion.1) | copy-start | bytes 393220
  153.3 26.2 %collective-permute-start = (f32[2,256]{1,0:T(2,128)S(1)}, f32[2,256]{1,0:T(2,128)S(1)}, u32[]{:S(2)}, u32[]{:S(2)}) collective-permute-start(f32[2,256]{1,0:T(2,128)S(1)} %slice.49), channel_id=1, source_target_pairs={{0,4},{4,8},{8,12},{12,16},{16,20},{20,24},{24,28},{1,5},{5,9},{9,... | collective-permute-start | bytes 6152 | tf_op jit(solution)/shard_map/ppermute | solution.py:10
  172.4 7.1 %copy-start.4 = (bf16[2048,256]{1,0:T(8,128)(2,1)S(1)}, bf16[2048,256]{1,0:T(8,128)(2,1)}, u32[]{:S(2)}) copy-start(bf16[2048,256]{1,0:T(8,128)(2,1)} %param.23) | copy-start | bytes 3145732
  172.4 7.1 %copy-start.11 = (f32[128,256]{1,0:T(8,128)S(1)}, f32[128,256]{1,0:T(8,128)}, u32[]{:S(2)}) copy-start(f32[128,256]{1,0:T(8,128)} %copy-done.10) | copy-start | bytes 393220
  172.4 7.1 %copy-start.12 = (bf16[128,256]{1,0:T(8,128)(2,1)S(1)}, bf16[128,256]{1,0:T(8,128)(2,1)}, u32[]{:S(2)}) copy-start(bf16[128,256]{1,0:T(8,128)(2,1)} %param.19) | copy-start | bytes 196612
  182.0 5.2 %copy-start.19 = (bf16[8,96,2048]{2,1,0:T(8,128)(2,1)S(1)}, bf16[8,96,2048]{2,1,0:T(8,128)(2,1)}, u32[]{:S(2)}) copy-start(bf16[8,96,2048]{2,1,0:T(8,128)(2,1)} %all-gather.5.cloned.1.call-done) | copy-start | bytes 9437188
  182.0 5.2 %copy-start.20 = (f32[768,512]{1,0:T(8,128)S(1)}, f32[768,512]{1,0:T(8,128)}, u32[]{:S(2)}) copy-start(f32[768,512]{1,0:T(8,128)} %fusion.5) | copy-start | bytes 4718596
  182.1 5.2 %copy-start.21 = (f32[768,512]{1,0:T(8,128)S(1)}, f32[768,512]{1,0:T(8,128)}, u32[]{:S(2)}) copy-start(f32[768,512]{1,0:T(8,128)} %fusion.8) | copy-start | bytes 4718596
  187.3 4.8 %copy-start.6 = (bf16[768,512]{1,0:T(8,128)(2,1)S(1)}, bf16[768,512]{1,0:T(8,128)(2,1)}, u32[]{:S(2)}) copy-start(bf16[768,512]{1,0:T(8,128)(2,1)} %copy-done.5) | copy-start | bytes 2359300
  187.3 4.8 %copy-start.18 = (bf16[8,96,2048]{2,1,0:T(8,128)(2,1)S(1)}, bf16[8,96,2048]{2,1,0:T(8,128)(2,1)}, u32[]{:S(2)}) copy-start(bf16[8,96,2048]{2,1,0:T(8,128)(2,1)} %all-gather.3.cloned.1.call-done) | copy-start | bytes 9437188
  190.6 5.6 %copy-start.13 = (bf16[128,256]{1,0:T(8,128)(2,1)S(1)}, bf16[128,256]{1,0:T(8,128)(2,1)}, u32[]{:S(2)}) copy-start(bf16[128,256]{1,0:T(8,128)(2,1)} %param.20) | copy-start | bytes 196612
  190.6 6.3 %copy-start.14 = (bf16[128,256]{1,0:T(8,128)(2,1)S(1)}, bf16[128,256]{1,0:T(8,128)(2,1)}, u32[]{:S(2)}) copy-start(bf16[128,256]{1,0:T(8,128)(2,1)} %param.21) | copy-start | bytes 196612
  190.6 5.6 %collective-permute-start.1 = (f32[2,256]{1,0:T(2,128)S(1)}, f32[2,256]{1,0:T(2,128)S(1)}, u32[]{:S(2)}, u32[]{:S(2)}) collective-permute-start(f32[2,256]{1,0:T(2,128)S(1)} %slice.54), channel_id=1, source_target_pairs={{4,0},{8,4},{12,8},{16,12},{20,16},{24,20},{28,24},{5,1},{9,5},{13... | collective-permute-start | bytes 6152 | tf_op jit(solution)/shard_map/ppermute | solution.py:10
  (5 other events, 10.8 us)
Sparse Core Ops, SparseCore 0:
  39.9 27.5 all-gather.2
  69.0 28.4 all-gather.4
  109.1 37.7 reduce-scatter.2
  182.1 62.8 reduce-scatter.4
where the time goes:
time: 254 us; the launch traced here: 253 us
  waiting for transfers between devices  127 us (50%)
  blocking collectives  57.3 us (23%)
  matrix products  34.8 us (14%)
  between operations  14.1 us (6%)
  starting transfers between devices  11 us (4%)
  other arithmetic  6.23 us (2%)
    reduce_scatter x1, waiting for transfers between devices, per_device(): lax.psum_scatter(lax.dot_general(stream_grad, conv_out, contract_first, p...  47.4 us
    reduce_scatter x1, waiting for transfers between devices, per_device(): lax.psum_scatter(row_partial.astype(jnp.bfloat16), 'tp', scatter_dimensio...  37.9 us
    all_to_all x1, blocking collectives, per_device(): lax.all_to_all(sent_rows, 'sp', split_axis=0, concat_axis=0, tiled=True)  27.3 us
    all_to_all x1, blocking collectives, per_device(): lax.all_to_all(sent_cot, 'sp', split_axis=0, concat_axis=0, tiled=True)  23.3 us
    all_gather x1, waiting for transfers between devices, per_device(): lax.all_gather(recv_cot, 'tp', axis=2, tiled=True)  22.2 us
    all_to_all x1, waiting for transfers between devices, per_device(): lax.all_to_all(half_grad, 'sp', split_axis=0, concat_axis=0, tiled=True)  15.2 us
    all_gather x1, blocking collectives, per_device(): moe_grad = lax.all_gather(moe_part, 'tp', axis=1, tiled=True)  6.68 us
    dot_general x1, matrix products, per_device(): lax.dot_general(routed_cot, down_local, contract_last, preferred_element_...  5.69 us
  transfers between devices with their start and end apart: 7, of which 6 were waited for; matrix products, arithmetic and copies ran while one was open for 9% of the time, Pallas kernels for 0%

commit v1 on v0

--- a/solution.py
+++ b/solution.py
@@ -2,6 +2,13 @@
 import jax.numpy as jnp
 from jax import lax
 from jax.sharding import PartitionSpec as P
+
+
+def pack_marks_in(s0, pos_dim):
+    s0 = jnp.moveaxis(s0, 0, pos_dim)
+    g_now = s0.shape
+    built = s0.reshape(*g_now[:pos_dim], g_now[pos_dim] * g_now[pos_dim + 1], *g_now[pos_dim + 2 :])
+    return built
 
 
 def from_behind(block, axis, distance):
@@ -58,9 +65,23 @@
         lax.all_to_all(sent_rows, "sp", split_axis=0, concat_axis=0, tiled=True),
         lax.all_to_all(sent_cot, "sp", split_axis=0, concat_axis=0, tiled=True),
     )
+
+    def connect_roots(raw, along_axis, out_dim):
+        n_all = jax.lax.psum(1, along_axis)
+        block_list = [raw]
+        nodes = tuple(((no, (no + 1) % n_all) for no in range(n_all)))
+        while len(block_list) < n_all:
+            prior = jax.lax.ppermute(block_list[-1], along_axis, nodes)
+            block_list.append(prior)
+        block_last = jax.lax.axis_index(along_axis)
+        tile_out = jnp.stack(block_list, axis=0)
+        block_list = tile_out[(block_last - jnp.arange(n_all)) % n_all]
+        step_out = pack_marks_in(block_list, out_dim)
+        return step_out
+
     recv_rows, recv_cot = (
         lax.all_gather(recv_rows, "tp", axis=2, tiled=True),
-        lax.all_gather(recv_cot, "tp", axis=2, tiled=True),
+        connect_roots(recv_cot, "tp", 2),
     )
     slots = groups * capacity
     routed_rows = recv_rows.reshape(slots, model_width)

time: 254 us -> 270 us (1.063)
  local copies, waits for them, and re-layouts: 2.48 us -> 15.4 us
  waiting for transfers between devices: 127 us -> 135 us
  matrix products: 34.8 us -> 29.2 us
    ppermute x0 -> x3, waiting for transfers between devices: none -> 34.2 us  [connect_roots(): prior = jax.lax.ppermute(block_list[-1], along_axis, nodes)]
    all_gather x1 -> x0, waiting for transfers between devices: 22.2 us -> none  [per_device(): lax.all_gather(recv_cot, 'tp', axis=2, tiled=True)]
    gather x0 -> x1, local copies, waits for them, and re-layouts: none -> 4.36 us  [connect_roots(): block_list = tile_out[(block_last - jnp.arange(n_all)) % n_all]]
    transpose x0 -> x1, local copies, waits for them, and re-layouts: none -> 4.32 us  [pack_marks_in(): s0 = jnp.moveaxis(s0, 0, pos_dim)]
    unnamed x46 -> x51, local copies, waits for them, and re-layouts: 1.45 us -> 5.69 us
    all_gather x1, waiting for transfers between devices: 3.51 us -> 0.01 us  [per_device(): lax.all_gather(recv_rows, 'tp', axis=2, tiled=True)]
    dot_general x1, matrix products: 5.69 us -> 2.31 us  [per_device(): lax.dot_general(routed_cot, down_local, contract_last, preferred_element_...]
  transfers between devices with their start and end apart: 7 -> 9, of which waited for: 6 -> 7; matrix products, arithmetic and copies ran while one was open for 9% -> 10% of each run, Pallas kernels for 0% -> 0%
where the time goes in v1:
time: 270 us
  waiting for transfers between devices  135 us (50%)
  blocking collectives  57.2 us (21%)
  matrix products  29.2 us (11%)
  local copies, waits for them, and re-layouts  15.4 us (6%)
  between operations  14.1 us (5%)
  starting transfers between devices  10.9 us (4%)
  other arithmetic  8.15 us (3%)
    reduce_scatter x1, waiting for transfers between devices, per_device(): lax.psum_scatter(lax.dot_general(stream_grad, conv_out, contract_first, p...  47.5 us
    reduce_scatter x1, waiting for transfers between devices, per_device(): lax.psum_scatter(row_partial.astype(jnp.bfloat16), 'tp', scatter_dimensio...  37 us
    ppermute x3, waiting for transfers between devices, connect_roots(): prior = jax.lax.ppermute(block_list[-1], along_axis, nodes)  34.2 us
    all_to_all x1, blocking collectives, per_device(): lax.all_to_all(sent_rows, 'sp', split_axis=0, concat_axis=0, tiled=True)  27.3 us
    all_to_all x1, blocking collectives, per_device(): lax.all_to_all(sent_cot, 'sp', split_axis=0, concat_axis=0, tiled=True)  23.2 us
    all_to_all x1, waiting for transfers between devices, per_device(): lax.all_to_all(half_grad, 'sp', split_axis=0, concat_axis=0, tiled=True)  15.2 us
    all_gather x1, blocking collectives, per_device(): moe_grad = lax.all_gather(moe_part, 'tp', axis=1, tiled=True)  6.68 us
    unnamed x51, local copies, waits for them, and re-layouts  5.69 us
  transfers between devices with their start and end apart: 9, of which 7 were waited for; matrix products, arithmetic and copies ran while one was open for 10% of the time, Pallas kernels for 0%

profile of v1, /device:TPU:0, one launch (start us, length us, event | category | flops | bytes accessed | tf_op | source)
XLA Modules:
  0.0 269.9 jit_solution(2896088067994891334)
XLA Ops:
  12.4 27.3 %all_to_all.15 = bf16[8,96,512]{2,1,0:T(8,128)(2,1)} all-to-all(bf16[8,96,512]{2,1,0:T(8,128)(2,1)S(1)} %bitcast.87), channel_id=1, replica_groups=mesh['sp'=8,'tp'=4] {'sp'}, dimensions={0} | all-to-all | bytes 1572864 | tf_op jit(solution)/shard_map/all_to_all | solution.py:65
  40.5 23.2 %all_to_all.16 = bf16[8,96,512]{2,1,0:T(8,128)(2,1)S(1)} all-to-all(bf16[8,96,512]{2,1,0:T(8,128)(2,1)S(1)} %bitcast.88), channel_id=1, replica_groups=mesh['sp'=8,'tp'=4] {'sp'}, dimensions={0} | all-to-all | bytes 1572864 | tf_op jit(solution)/shard_map/all_to_all | solution.py:66
  63.7 11.4 %collective-permute-done = bf16[8,96,512]{2,1,0:T(8,128)(2,1)S(1)} collective-permute-done((bf16[8,96,512]{2,1,0:T(8,128)(2,1)S(1)}, bf16[8,96,512]{2,1,0:T(8,128)(2,1)S(1)}, u32[]{:S(2)}, u32[]{:S(2)}) %collective-permute-start) | collective-permute-done | bytes 786464 | tf_op jit(solution)/shard_map/ppermute | solution.py:74
  75.2 11.4 %collective-permute-done.1 = bf16[8,96,512]{2,1,0:T(8,128)(2,1)S(1)} collective-permute-done((bf16[8,96,512]{2,1,0:T(8,128)(2,1)S(1)}, bf16[8,96,512]{2,1,0:T(8,128)(2,1)S(1)}, u32[]{:S(2)}, u32[]{:S(2)}) %collective-permute-start.1) | collective-permute-done | bytes 786464 | tf_op jit(solution)/shard_map/ppermute | solution.py:74
  86.6 11.4 %collective-permute-done.2 = bf16[8,96,512]{2,1,0:T(8,128)(2,1)S(1)} collective-permute-done((bf16[8,96,512]{2,1,0:T(8,128)(2,1)S(1)}, bf16[8,96,512]{2,1,0:T(8,128)(2,1)S(1)}, u32[]{:S(2)}, u32[]{:S(2)}) %collective-permute-start.2) | collective-permute-done | bytes 786464 | tf_op jit(solution)/shard_map/ppermute | solution.py:74
  98.0 1.9 pad_maximum_fusion
  99.9 4.4 %gather_fusion = bf16[4,8,96,512]{3,2,1,0:T(8,128)(2,1)} fusion(bf16[4,8,96,512]{3,2,1,0:T(8,128)(2,1)} %pad_maximum_fusion, s32[1024]{0:T(1024)S(1)} %pad_clamp_fusion), kind=kCustom, calls=%fused_computation | custom fusion | bytes 6291472 | tf_op jit(solution)/shard_map/gather | solution.py:78
  104.2 4.3 %copy.52 = bf16[8,96,4,512]{3,2,1,0:T(4,128)(2,1)S(1)} copy(bf16[8,96,4,512]{3,1,0,2:T(8,128)(2,1)} %bitcast.82) | data formatting | bytes 6291456 | tf_op jit(solution)/shard_map/transpose | solution.py:8
  108.6 2.7 copy.54
  111.3 3.8 %fusion.5 = f32[768,512]{1,0:T(8,128)S(1)} fusion(bf16[768,2048]{1,0:T(8,128)(2,1)} %bitcast.103, bf16[1,2048,512]{2,1,0:T(8,128)(2,1)S(1)} %copy-done), kind=kOutput, calls=%fused_computation.12 | convolution fusion | flops 1610612736 | bytes 6815744 | tf_op jit(solution)/shard_map/dot_general | solution.py:92
  115.1 1.8 fusion.8
  118.8 2.3 multiply_convert_fusion.1
  121.1 1.8 fusion.3
  123.0 3.5 %add_convert_fusion = bf16[768,2048]{1,0:T(8,128)(2,1)} fusion(f32[768,2048]{1,0:T(8,128)S(1)} %fusion.3, bf16[768,512]{1,0:T(8,128)(2,1)S(1)} %get-tuple-element.11, bf16[1,2048,512]{2,1,0:T(8,128)(2,1)S(1)} %copy-done.4), kind=kOutput, calls=%fused_computation.1 | convolution fusion | flops 1613758464 | bytes 12320768 | tf_op jit(solution)/shard_map/dot_general | solution.py:116
  126.6 37.0 %reduce-scatter.3.cloned.1.call-done = bf16[768,512]{1,0:T(8,128)(2,1)} async-done(((bf16[768,2048]{1,0:T(8,128)(2,1)}), bf16[768,512]{1,0:T(8,128)(2,1)}) %reduce-scatter.3.cloned.1.call-update) | async-done | bytes 786448 | tf_op jit(solution)/shard_map/reduce_scatter | solution.py:119
  163.6 5.5 %all-to-all-start.2 = ((bf16[8,96,512]{2,1,0:T(8,128)(2,1)}), bf16[8,96,512]{2,1,0:T(8,128)(2,1)S(1)}, u32[]{:S(2)}, u32[]{:S(2)}) async-start(bf16[8,96,512]{2,1,0:T(8,128)(2,1)} %bitcast.95), calls=%async_computation.3 | async-start | bytes 1572864 | tf_op jit(solution)/shard_map/all_to_all | solution.py:124
  170.0 3.9 %collective-permute-start.3 = (f32[2,256]{1,0:T(2,128)S(1)}, f32[2,256]{1,0:T(2,128)S(1)}, u32[]{:S(2)}, u32[]{:S(2)}) collective-permute-start(f32[2,256]{1,0:T(2,128)S(1)} %slice.51), channel_id=1, source_target_pairs={{0,4},{4,8},{8,12},{12,16},{16,20},{20,24},{24,28},{1,5},{5,9},{9,... | collective-permute-start | bytes 6152 | tf_op jit(solution)/shard_map/ppermute | solution.py:17
  174.0 15.2 %all-to-all-done.2 = bf16[8,96,512]{2,1,0:T(8,128)(2,1)S(1)} async-done(((bf16[8,96,512]{2,1,0:T(8,128)(2,1)}), bf16[8,96,512]{2,1,0:T(8,128)(2,1)S(1)}, u32[]{:S(2)}, u32[]{:S(2)}) %all-to-all-start.2) | async-done | bytes 786464 | tf_op jit(solution)/shard_map/all_to_all | solution.py:124
  189.5 6.7 %all_gather.7 = bf16[128,2048]{1,0:T(8,128)(2,1)S(1)} all-gather(bf16[128,512]{1,0:T(8,128)(2,1)S(1)} %fusion.14), channel_id=1, replica_groups=mesh['sp'=8,'tp'=4] {'tp'}, dimensions={1}, use_global_device_ids=true | all-gather | bytes 655360 | tf_op jit(solution)/shard_map/all_gather | solution.py:130
  198.8 5.2 %fusion = bf16[1,2048,512]{2,1,0:T(8,128)(2,1)} fusion(bf16[768,2048]{1,0:T(8,128)(2,1)} %bitcast.104, bf16[768,512]{1,0:T(8,128)(2,1)S(1)} %copy-done.9), kind=kOutput, calls=%fused_computation.6 | convolution fusion | flops 1611661312 | bytes 6029312 | tf_op jit(solution)/shard_map/dot_general | solution.py:104
  204.0 3.3 %fusion.2 = bf16[1,512,2048]{2,1,0:T(8,128)(2,1)} fusion(bf16[768,2048]{1,0:T(8,128)(2,1)S(1)} %bitcast.86, f32[768,512]{1,0:T(8,128)S(1)} %copy-done.23, f32[768,512]{1,0:T(8,128)S(1)} %copy-done.21), kind=kOutput, calls=%fused_computation.8 | convolution fusion | flops 1614020608 | bytes 8388608 | tf_op jit(solution)/shard_map/dot_general | solution.py:110
  208.8 3.2 %fusion.1 = bf16[1,2048,512]{2,1,0:T(8,128)(2,1)} fusion(bf16[768,2048]{1,0:T(8,128)(2,1)S(1)} %bitcast.106, bf16[768,512]{1,0:T(8,128)(2,1)S(1)} %copy-done.7), kind=kOutput, calls=%fused_computation.7 | convolution fusion | flops 1611661312 | bytes 6029312 | tf_op jit(solution)/shard_map/dot_general | solution.py:107
  214.3 47.5 %reduce-scatter.5.cloned.1.call-done = bf16[256,256]{1,0:T(8,128)(2,1)} async-done(((bf16[2048,256]{1,0:T(8,128)(2,1)}), bf16[256,256]{1,0:T(8,128)(2,1)}) %reduce-scatter.5.cloned.1.call-update) | async-done | bytes 131088 | tf_op jit(solution)/shard_map/reduce_scatter | solution.py:143
  261.7 1.6 convert_element_type.125
  (97 shorter events, 15.4 us)
Async XLA Ops:
  7.2 104.1 %copy-start = (bf16[1,2048,512]{2,1,0:T(8,128)(2,1)S(1)}, bf16[1,2048,512]{2,1,0:T(8,128)(2,1)}, u32[]{:S(2)}) copy-start(bf16[1,2048,512]{2,1,0:T(8,128)(2,1)} %param.16) | copy-start | bytes 6291460
  7.2 104.1 %all-gather.2.cloned.1.call-start = ((), (), s32[]{:S(2)}) async-start(), calls=%async_computation.5 | async-start | bytes 3932160 | tf_op jit(solution)/shard_map/all_gather | solution.py:83
  11.1 28.7 %copy-start.16 = (f32[128,2]{0,1:T(2,128)S(1)}, f32[128,2]{0,1:T(2,128)}, u32[]{:S(2)}) copy-start(f32[128,2]{0,1:T(2,128)} %param.15) | copy-start | bytes 3076
  11.1 29.1 %copy-start.3 = (bf16[128,2048]{1,0:T(8,128)(2,1)S(1)}, bf16[128,2048]{1,0:T(8,128)(2,1)}, u32[]{:S(2)}) copy-start(bf16[128,2048]{1,0:T(8,128)(2,1)} %param.12) | copy-start | bytes 1572868
  39.7 123.8 %reduce-scatter.3.cloned.1.call-start = ((), (), s32[]{:S(2)}) async-start(), calls=%async_computation.6 | async-start | bytes 3932160 | tf_op jit(solution)/shard_map/reduce_scatter | solution.py:119
  63.7 11.4 %collective-permute-start = (bf16[8,96,512]{2,1,0:T(8,128)(2,1)S(1)}, bf16[8,96,512]{2,1,0:T(8,128)(2,1)S(1)}, u32[]{:S(2)}, u32[]{:S(2)}) collective-permute-start(bf16[8,96,512]{2,1,0:T(8,128)(2,1)S(1)} %all_to_all.16), channel_id=1, source_target_pairs={{0,1},{1,2},{2,3},{3,0},{4,5},{5,6},{6,7},{7,4},{8,9},{9,10},{10,1... | collective-permute-start | bytes 2359304 | tf_op jit(solution)/shard_map/ppermute | solution.py:74
  75.2 11.4 %collective-permute-start.1 = (bf16[8,96,512]{2,1,0:T(8,128)(2,1)S(1)}, bf16[8,96,512]{2,1,0:T(8,128)(2,1)S(1)}, u32[]{:S(2)}, u32[]{:S(2)}) collective-permute-start(bf16[8,96,512]{2,1,0:T(8,128)(2,1)S(1)} %collective-permute-done), channel_id=1, source_target_pairs={{0,1},{1,2},{2,3},{3,0},{4,5},{5,6},{6,7},{7,4},{8,9},{9,10},{10,1... | collective-permute-start | bytes 2359304 | tf_op jit(solution)/shard_map/ppermute | solution.py:74
  86.6 11.4 %collective-permute-start.2 = (bf16[8,96,512]{2,1,0:T(8,128)(2,1)S(1)}, bf16[8,96,512]{2,1,0:T(8,128)(2,1)S(1)}, u32[]{:S(2)}, u32[]{:S(2)}) collective-permute-start(bf16[8,96,512]{2,1,0:T(8,128)(2,1)S(1)} %collective-permute-done.1), channel_id=1, source_target_pairs={{0,1},{1,2},{2,3},{3,0},{4,5},{5,6},{6,7},{7,4},{8,9},{9,10},{10,1... | collective-permute-start | bytes 2359304 | tf_op jit(solution)/shard_map/ppermute | solution.py:74
  116.9 4.2 %copy-start.22 = (f32[768,512]{1,0:T(8,128)}, f32[768,512]{1,0:T(8,128)S(1)}, u32[]{:S(2)}) copy-start(f32[768,512]{1,0:T(8,128)S(1)} %fusion.8) | copy-start | bytes 4718596
  126.5 47.4 %copy-start.15 = (bf16[3,256]{1,0:T(4,128)(2,1)S(1)}, bf16[3,256]{1,0:T(4,128)(2,1)}, u32[]{:S(2)}) copy-start(bf16[3,256]{1,0:T(4,128)(2,1)} %param.22) | copy-start | bytes 4612
  163.6 25.6 %all-to-all-start.2 = ((bf16[8,96,512]{2,1,0:T(8,128)(2,1)}), bf16[8,96,512]{2,1,0:T(8,128)(2,1)S(1)}, u32[]{:S(2)}, u32[]{:S(2)}) async-start(bf16[8,96,512]{2,1,0:T(8,128)(2,1)} %bitcast.95), calls=%async_computation.3 | async-start | bytes 1572864 | tf_op jit(solution)/shard_map/all_to_all | solution.py:124
  169.1 92.6 %reduce-scatter.5.cloned.1.call-start = ((), (), s32[]{:S(2)}) async-start(), calls=%async_computation.7 | async-start | bytes 1179648 | tf_op jit(solution)/shard_map/reduce_scatter | solution.py:143
  170.0 26.2 %collective-permute-start.3 = (f32[2,256]{1,0:T(2,128)S(1)}, f32[2,256]{1,0:T(2,128)S(1)}, u32[]{:S(2)}, u32[]{:S(2)}) collective-permute-start(f32[2,256]{1,0:T(2,128)S(1)} %slice.51), channel_id=1, source_target_pairs={{0,4},{4,8},{8,12},{12,16},{16,20},{20,24},{24,28},{1,5},{5,9},{9,... | collective-permute-start | bytes 6152 | tf_op jit(solution)/shard_map/ppermute | solution.py:17
  189.2 7.1 %copy-start.5 = (bf16[2048,256]{1,0:T(8,128)(2,1)S(1)}, bf16[2048,256]{1,0:T(8,128)(2,1)}, u32[]{:S(2)}) copy-start(bf16[2048,256]{1,0:T(8,128)(2,1)} %param.23) | copy-start | bytes 3145732
  189.2 7.1 %copy-start.11 = (f32[128,256]{1,0:T(8,128)S(1)}, f32[128,256]{1,0:T(8,128)}, u32[]{:S(2)}) copy-start(f32[128,256]{1,0:T(8,128)} %copy-done.10) | copy-start | bytes 393220
  189.2 7.1 %copy-start.12 = (bf16[128,256]{1,0:T(8,128)(2,1)S(1)}, bf16[128,256]{1,0:T(8,128)(2,1)}, u32[]{:S(2)}) copy-start(bf16[128,256]{1,0:T(8,128)(2,1)} %param.19) | copy-start | bytes 196612
  198.7 5.2 %copy-start.2 = (bf16[96,8,4,512]{3,1,2,0:T(8,128)(2,1)S(1)}, bf16[96,8,4,512]{3,1,2,0:T(8,128)(2,1)}, u32[]{:S(2)}) copy-start(bf16[96,8,4,512]{3,1,2,0:T(8,128)(2,1)} %copy.54) | copy-start | bytes 9437188
  198.7 5.2 %copy-start.21 = (f32[768,512]{1,0:T(8,128)S(1)}, f32[768,512]{1,0:T(8,128)}, u32[]{:S(2)}) copy-start(f32[768,512]{1,0:T(8,128)} %copy-done.20) | copy-start | bytes 4718596
  198.7 5.2 %copy-start.23 = (f32[768,512]{1,0:T(8,128)S(1)}, f32[768,512]{1,0:T(8,128)}, u32[]{:S(2)}) copy-start(f32[768,512]{1,0:T(8,128)} %copy-done.22) | copy-start | bytes 4718596
  204.0 4.8 %copy-start.7 = (bf16[768,512]{1,0:T(8,128)(2,1)S(1)}, bf16[768,512]{1,0:T(8,128)(2,1)}, u32[]{:S(2)}) copy-start(bf16[768,512]{1,0:T(8,128)(2,1)} %copy-done.6) | copy-start | bytes 2359300
  204.0 4.8 %copy-start.18 = (bf16[8,96,2048]{2,1,0:T(8,128)(2,1)S(1)}, bf16[8,96,2048]{2,1,0:T(8,128)(2,1)}, u32[]{:S(2)}) copy-start(bf16[8,96,2048]{2,1,0:T(8,128)(2,1)} %all-gather.2.cloned.1.call-done) | copy-start | bytes 9437188
  207.3 5.6 %copy-start.13 = (bf16[128,256]{1,0:T(8,128)(2,1)S(1)}, bf16[128,256]{1,0:T(8,128)(2,1)}, u32[]{:S(2)}) copy-start(bf16[128,256]{1,0:T(8,128)(2,1)} %param.20) | copy-start | bytes 196612
  207.3 6.3 %copy-start.14 = (bf16[128,256]{1,0:T(8,128)(2,1)S(1)}, bf16[128,256]{1,0:T(8,128)(2,1)}, u32[]{:S(2)}) copy-start(bf16[128,256]{1,0:T(8,128)(2,1)} %param.21) | copy-start | bytes 196612
  207.3 5.6 %collective-permute-start.4 = (f32[2,256]{1,0:T(2,128)S(1)}, f32[2,256]{1,0:T(2,128)S(1)}, u32[]{:S(2)}, u32[]{:S(2)}) collective-permute-start(f32[2,256]{1,0:T(2,128)S(1)} %slice.56), channel_id=1, source_target_pairs={{4,0},{8,4},{12,8},{16,12},{20,16},{24,20},{28,24},{5,1},{9,5},{13... | collective-permute-start | bytes 6152 | tf_op jit(solution)/shard_map/ppermute | solution.py:17
  (9 other events, 24.8 us)
Sparse Core Ops, SparseCore 0:
  39.9 27.5 all-gather.1
  126.7 36.8 reduce-scatter.2
  198.8 62.8 reduce-scatter.4
